TPU v7x, 32 devices: a whole 2x2x4 slice. The times are simulated.
32 devices in a mesh: sp: 16 (over z, y, x), tp: 2 (over core).
Axes of the slice: x: 2, y: 2, z: 4, core: 2. Of those that a mesh axis runs over, the one named last changes fastest.
Arguments:
- query_logits: bfloat16 [2048, 1024], P('sp', 'tp'), may hold values from -6 to 6
- value_rows: bfloat16 [2048, 1024], P('sp', 'tp'), may hold values from -6 to 6
- onward_forget_logits: bfloat16 [2048, 1024], P('sp', 'tp'), may hold values from -5.5 to 5.5
- reverse_forget_logits: bfloat16 [2048, 1024], P('sp', 'tp'), may hold values from -5.5 to 5.5
- output_gate_logits: bfloat16 [2048, 1024], P('sp', 'tp'), may hold values from -6 to 6
- onward_floor_gap: float32 [1024], P('tp'), may hold values from 0 to 0.12, as said below
- reverse_floor_gap: float32 [1024], P('tp'), may hold values from 0 to 0.12, as said below
- extra_log_decay: float32 [2048, 8], P('sp', 'tp'), may hold values from -2.1 to 0
- per_head_gain: float32 [128], replicated, may hold values from 0.1 to 1.9
- residual: bfloat16 [2048, 2048], P('sp', 'tp'), may hold values from -8 to 8
- output_matrix: bfloat16 [1024, 2048], P(None, 'tp'), may hold values from -0.375 to 0.375
- inner_norm_gain: float32 [2048], P('tp'), may hold values from 0.1 to 1.9
- inner_norm_bias: float32 [2048], P('tp'), may hold values from -1.5 to 1.5
- gate_matrix: bfloat16 [2048, 5632], P('sp', 'tp'), may hold values from -0.125 to 0.125
- up_matrix: bfloat16 [2048, 5632], P('sp', 'tp'), may hold values from -0.125 to 0.125
- down_matrix: bfloat16 [5632, 2048], P('tp', 'sp'), may hold values from -0.15625 to 0.15625
- closing_norm_gain: float32 [2048], P('tp'), may hold values from 0.1 to 1.9
- closing_norm_bias: float32 [2048], P('tp'), may hold values from -1.5 to 1.5
Outputs:
- layer_output: bfloat16 [2048, 2048], P('sp', 'tp')
Inputs may be any that keep to these rules, and one draw needn't show every extreme that they name: `onward_floor_gap`: positive. `reverse_floor_gap`: positive.
All inputs are finite; a program needn't handle non-finite values.
Results may differ from a plain program's by a relative error of at most 0.014.
Values may be sent and summed in bfloat16 or wider, within the bound.
A program may use at most 128 MiB of HBM per device.

v0:
```python
import functools
import math

import jax
import jax.numpy as jnp
from jax import lax
from jax.experimental import pallas as pl
from jax.experimental.pallas import tpu as pltpu
from jax.sharding import PartitionSpec as P

highest = lax.Precision.HIGHEST
alpha_mix = 2.0**0.25
norm_eps = 1e-05
head_eps = 1e-06
bf16 = jnp.bfloat16
f32 = jnp.float32
MESH = pl.DeviceIdType.MESH


def pick(table, at):
    out = jnp.int32(table[0])
    for i, value in enumerate(table[1:], 1):
        out = jnp.where(at == i, jnp.int32(value), out)
    return out


def across(x, w):
    return lax.dot_general(x, w, (((1,), (1,)), ((), ())), preferred_element_type=f32)


def silu(x):
    return x / (1.0 + jnp.exp(-x))


def layer_kernel(
    far, near, cores,
    q_ref, v_ref, f_ref, r_ref, og_ref, fg_ref, rg_ref, ex_ref, hg_ref, res_ref, om_ref, ig_ref,
    ib_ref, gate_ref, up_ref, down_ref, cg_ref, cb_ref, out_ref,
    wbuf, dbuf, wsend, st_send, tot_send, st_recv, tot_recv, fs_send, ft_send, f_recv, ft_recv,
    b_send, b_recv, om_all, res_all, ig_all, ib_all, g_all, x_all, inner, dq, hid, ts_send,
    ts_recv, rs_send, rs_recv, fin_all, xs,
    deal_s, deal_r, ring_s, ring_r, s1_s, s1_r, s2_s, s2_r, s3_s, s3_r, tp_s, tp_r, ga_s, ga_r,
    ag_s, ag_r, d2_s, d2_r, ts_s, ts_r, rs_s, rs_r, fin_s, fin_r, own_s,
):
    rows = q_ref.shape[0]
    heads, width = ex_ref.shape[1], hg_ref.shape[1]
    units, deep = dbuf.shape[2:]
    chunk = st_send.shape[2]
    per_head = near // heads
    share = near // cores
    half = (units // 2 + 15) // 16 * 16
    n2 = near // 2
    me, core = lax.axis_index("sp"), lax.axis_index("tp")
    z, p = me // near, me % near

    ring = [i ^ (i >> 1) for i in range(near)]
    spot = [ring.index(i) for i in range(near)]
    right = pick([ring[(spot[i] + 1) % near] for i in range(near)], p)
    left = pick([ring[(spot[i] - 1) % near] for i in range(near)], p)

    def behind(sign, d):
        return pick([ring[(spot[i] - sign * d) % near] for i in range(near)], p)

    partners = [sorted((j for j in range(far) if j != i), key=lambda j: (abs(j - i), j))
                for i in range(far)]
    order = [z] + [pick([partners[i][k] for i in range(far)], z) for k in range(far - 1)]

    sends = []

    def copy(src, dst, ssem, rsem, to):
        return pltpu.make_async_remote_copy(
            src_ref=src, dst_ref=dst, send_sem=ssem, recv_sem=rsem, device_id=to,
            device_id_type=MESH,
        )

    def start(c, when=None):
        sends.append((c, when))
        if when is None:
            c.start()
        else:
            pl.when(when)(c.start)

    def landed(c, when=None):
        if when is None:
            c.wait_recv()
        else:
            pl.when(when)(c.wait_recv)

    def at(zz, pp):
        return (zz * near + pp, core)

    def mate(m):
        return (me, (core + m) % cores)

    f_recv[...] = jnp.zeros_like(f_recv)
    ft_recv[...] = jnp.zeros_like(ft_recv)

    barrier = pltpu.get_barrier_semaphore()
    peers = [at(z, (p + j) % near) for j in range(1, near)]
    peers += [at((z + j) % far, p) for j in range(1, far)]
    peers += [mate(m) for m in range(1, cores)]
    for peer in peers:
        pl.semaphore_signal(barrier, inc=1, device_id=peer, device_id_type=MESH)

    own_om = pltpu.make_async_copy(om_ref, om_all.at[core], own_s.at[0])
    own_om.start()
    for i, ref in enumerate((gate_ref, up_ref)):
        whole = ref[...].astype(f32).T
        for j in range(far):
            wsend[j, i] = whole[j * units : (j + 1) * units].astype(bf16)
    wbuf[p, z] = wsend[z]
    dbuf[p, z] = down_ref[pl.ds(pl.multiple_of(z * units, 16), units), :]
    res_all[core] = res_ref[...]
    ig_all[core] = ig_ref[...]
    ib_all[core] = ib_ref[...]
    pl.semaphore_wait(barrier, len(peers))

    def deal_copy(g, k, out):
        zz = order[k + 1]
        if g == 0:
            src, dst = wsend.at[zz], wbuf
        else:
            src, dst = down_ref.at[pl.ds(pl.multiple_of(zz * units, 16), units), :], dbuf
        slot = z if out else zz
        return copy(src, dst.at[p, slot], deal_s.at[g, k], deal_r.at[g, slot], at(zz, p))

    def deal(g, k):
        start(deal_copy(g, k, True))

    def ring_copy(k, sign, d, block):
        g, zz = k // far, order[k % far]
        buf = dbuf if g else wbuf
        side = 0 if sign > 0 else 1
        ref = buf.at[block, zz]
        if d == n2:
            if g:
                ref = ref.at[pl.ds(0, half), :] if side == 0 else ref.at[pl.ds(half, units - half), :]
            else:
                ref = ref.at[pl.ds(side, 1)]
        to = right if sign > 0 else left
        return copy(ref, ref, ring_s.at[side, d - 1, k], ring_r.at[side, d - 1, k], at(z, to))

    def ring_start(k):
        if k % far:
            landed(deal_copy(k // far, k % far - 1, False))
        for sign in (1, -1):
            start(ring_copy(k, sign, 1, p))

    def ring_forward(k):
        for d in range(1, n2):
            for sign in (1, -1):
                block = behind(sign, d)
                landed(ring_copy(k, sign, d, block))
                start(ring_copy(k, sign, d + 1, block))

    def ring_done(k):
        for sign in (1, -1):
            landed(ring_copy(k, sign, n2, behind(sign, n2)))

    for k in range(far - 1):
        deal(0, k)
    ring_start(0)

    pairs = ((om_ref, om_all), (res_ref, res_all), (ig_ref, ig_all), (ib_ref, ib_all))

    def tp_copy(i, m, out):
        src, dst = pairs[i]
        slot = core if out else (core + cores - m) % cores
        return copy(src, dst.at[slot], tp_s.at[i, m], tp_r.at[i, m], mate(m))

    for m in range(1, cores):
        for i in range(len(pairs)):
            start(tp_copy(i, m, True))

    t = lax.broadcasted_iota(jnp.int32, (rows, rows), 0)
    s = lax.broadcasted_iota(jnp.int32, (rows, rows), 1)
    lower, upper = s <= t, s >= t
    for h in range(heads):
        cols = slice(h * width, (h + 1) * width)
        q = silu(q_ref[:, cols].astype(f32))
        v = v_ref[:, cols]
        extra = ex_ref[:, h : h + 1]
        scores = jnp.zeros((rows, rows), f32)
        for d, (raw_ref, gap_ref, tri) in enumerate(
            ((f_ref, fg_ref, lower), (r_ref, rg_ref, upper))
        ):
            raw = raw_ref[:, cols].astype(f32)
            key = gap_ref[:, cols] * (1.0 / (1.0 + jnp.exp(raw)))
            log = jnp.log1p(-key) + extra
            run = jnp.dot(tri.astype(f32), log, precision=highest, preferred_element_type=f32)
            last = run[rows - 1 :, :] if d == 0 else run[:1, :]
            qd = (q * jnp.exp(run)).astype(bf16)
            ki = (key * jnp.exp(-run)).astype(bf16)
            ks = (key * jnp.exp(last - run)).astype(bf16)
            scores = scores + jnp.where(tri, across(qd, ki), 0.0)
            dq[d, :, cols] = qd
            state = lax.dot_general(v, ks, (((0,), (0,)), ((), ())), preferred_element_type=f32)
            for i in range(per_head):
                st_send[h * per_head + i, d] = state[i * chunk : (i + 1) * chunk].astype(bf16)
                tot_send[h * per_head + i, d] = last
        inner[:, cols] = jnp.dot(scores.astype(bf16), v, preferred_element_type=f32)

    def plane_copy(i, j, out):
        src, dst = ((st_send, st_recv), (tot_send, tot_recv))[i]
        to = (p + j) % near
        slot = p if out else (p + near - j) % near
        return copy(src.at[to], dst.at[slot], s1_s.at[i, j], s1_r.at[i, j], at(z, to))

    for j in range(1, near):
        for i in range(2):
            start(plane_copy(i, j, True))
    st_recv[p] = st_send[p]
    tot_recv[p] = tot_send[p]

    ring_forward(0)

    for j in range(1, near):
        for i in range(2):
            landed(plane_copy(i, j, False))

    prefix = [[None] * near, [None] * near]
    gone = [[None] * near, [None] * near]
    for d in range(2):
        state = jnp.zeros((chunk, width), f32)
        total = jnp.zeros((1, width), f32)
        for b in range(near) if d == 0 else reversed(range(near)):
            prefix[d][b], gone[d][b] = state, total
            step = tot_recv[b, d]
            state = state * jnp.exp(step) + st_recv[b, d].astype(f32)
            total = total + step
        fs_send[d] = state.astype(bf16)
        ft_send[d] = total

    def far_copy(i, d, e):
        src, dst = ((fs_send, f_recv), (ft_send, ft_recv))[i]
        to = (z + e) % far if d == 0 else (z + far - e) % far
        return copy(src.at[d], dst.at[d, e], s2_s.at[i, d, e], s2_r.at[i, d, e], at(to, p))

    def far_valid(d, e, out):
        return z + e < far if (d == 0) == out else z >= e

    for e in range(1, far):
        for d in range(2):
            for i in range(2):
                start(far_copy(i, d, e), far_valid(d, e, True))

    ring_start(1)

    for e in range(1, far):
        for d in range(2):
            for i in range(2):
                landed(far_copy(i, d, e), far_valid(d, e, False))

    for d in range(2):
        enter = jnp.zeros((chunk, width), f32)
        for e in reversed(range(1, far)):
            enter = enter * jnp.exp(ft_recv[d, e]) + f_recv[d, e].astype(f32)
        for b in range(near):
            b_send[b, d] = (enter * jnp.exp(gone[d][b]) + prefix[d][b]).astype(bf16)

    def back_copy(j, out):
        to = (p + j) % near
        slot = p if out else (p + near - j) % near
        return copy(b_send.at[to], b_recv.at[slot], s3_s.at[j], s3_r.at[j], at(z, to))

    for j in range(1, near):
        start(back_copy(j, True))
    b_recv[p] = b_send[p]

    ring_start(far)

    for j in range(1, near):
        landed(back_copy(j, False))

    for h in range(heads):
        cols = slice(h * width, (h + 1) * width)
        mixed = inner[:, cols]
        for d in range(2):
            state = jnp.concatenate(
                [b_recv[h * per_head + i, d].astype(f32) for i in range(per_head)], axis=0
            ).astype(bf16)
            mixed = mixed + across(dq[d, :, cols], state)
        normed = (
            mixed
            * lax.rsqrt(jnp.mean(mixed * mixed, axis=1, keepdims=True) + head_eps)
            * hg_ref[...]
        )
        g_all[core, :, cols] = (normed * silu(og_ref[:, cols].astype(f32))).astype(bf16)

    def gated_copy(m, out):
        slot = core if out else (core + cores - m) % cores
        return copy(g_all.at[slot], g_all.at[slot], ga_s.at[m], ga_r.at[m], mate(m))

    for m in range(1, cores):
        start(gated_copy(m, True))
    own_om.wait()
    for m in range(1, cores):
        for i in range(len(pairs)):
            landed(tp_copy(i, m, False))
    for m in range(1, cores):
        landed(gated_copy(m, False))

    span = q_ref.shape[1]
    parts = []
    for b in range(cores):
        mixer = alpha_mix * res_all[b].astype(f32)
        for m in range(cores):
            mixer = mixer + jnp.dot(
                g_all[m], om_all[b, m * span : (m + 1) * span, :], preferred_element_type=f32
            )
        parts.append(mixer)
    wide = parts[0].shape[1]
    model = cores * wide
    mean = sum(jnp.sum(x, axis=1, keepdims=True) for x in parts) / model
    parts = [x - mean for x in parts]
    var = sum(jnp.sum(x * x, axis=1, keepdims=True) for x in parts) / model
    scale = lax.rsqrt(var + norm_eps)
    for b, x in enumerate(parts):
        x_all[z, b] = (x * scale * ig_all[b] + ib_all[b]).astype(bf16)

    def line_copy(sign, d):
        block = (z + far + (1 - d) * sign) % far
        side = 0 if sign > 0 else 1
        ref = x_all.at[block, core]
        return copy(ref, ref, ag_s.at[side, d], ag_r.at[side, d], at((z + far + sign) % far, p))

    def line_land(sign, d):
        block = (z + far - d * sign) % far
        side = 0 if sign > 0 else 1
        ref = x_all.at[block, core]
        return copy(ref, ref, ag_s.at[side, d], ag_r.at[side, d], at((z + far + sign) % far, p))

    def line_out(sign, d):
        return jnp.logical_and(z + 1 < far, z >= d - 1) if sign > 0 else jnp.logical_and(z > 0, z + d - 1 < far)

    def line_in(sign, d):
        return z >= d if sign > 0 else z + d < far

    def line_share(sign, d, m, out):
        block = (z + far - d * sign) % far
        side = 0 if sign > 0 else 1
        slot = core if out else (core + cores - m) % cores
        ref = x_all.at[block, slot]
        return copy(ref, ref, d2_s.at[side, d, m], d2_r.at[side, d, m], mate(m))

    def line_step(d):
        for sign in (1, -1):
            landed(line_land(sign, d), line_in(sign, d))
            if d + 1 < far:
                start(line_copy(sign, d + 1), line_out(sign, d + 1))
            for m in range(1, cores):
                start(line_share(sign, d, m, True), line_in(sign, d))

    for sign in (1, -1):
        start(line_copy(sign, 1), line_out(sign, 1))
    ring_forward(1)
    ring_start(2)
    ring_forward(far)
    line_step(1)
    ring_forward(2)
    line_step(2)
    ring_start(3)
    deal(1, 0)
    for d in range(3, far):
        line_step(d)
    for k in range(1, far - 1):
        deal(1, k)
    ring_forward(3)
    for k in range(4, far):
        ring_start(k)
        ring_forward(k)
    for d in range(1, far):
        for sign in (1, -1):
            for m in range(1, cores):
                landed(line_share(sign, d, m, False), line_in(sign, d))
    ring_start(far + 1)
    for k in range(far):
        ring_done(k)

    step = 256
    for n0 in range(0, units, step):
        n1 = min(units, n0 + step)
        gate = up = 0.0
        for pp in range(near):
            spots = [(zz * near + pp) * deep for zz in range(far)]
            x = jnp.concatenate(
                [
                    jnp.concatenate(
                        [x_all[j, c // wide, :, c % wide : c % wide + deep] for c in spots], axis=1
                    )
                    for j in range(far)
                ],
                axis=0,
            )
            wg, wu = (
                jnp.concatenate([wbuf[pp, zz, i, n0:n1, :] for zz in range(far)], axis=1)
                for i in range(2)
            )
            gate = gate + across(x, wg)
            up = up + across(x, wu)
        hid[:, n0:n1] = (silu(gate) * up).astype(bf16)

    def sum_copy(k, m):
        return copy(
            ts_send.at[k, (core + m) % cores], ts_recv.at[k, m], ts_s.at[k, m], ts_r.at[k, m],
            mate(m),
        )

    def reduce_copy(k, j, out):
        zz, to = order[k], order[j + 1]
        src, dst = rs_send.at[k, to], rs_recv.at[z, zz]
        return copy(src, dst, rs_s.at[k, j], rs_r.at[zz, z], at(to, p))

    def down(k):
        zz = order[k]
        w = jnp.concatenate([dbuf[pp, zz] for pp in range(near)], axis=1)
        y = jnp.dot(hid[...], w, preferred_element_type=f32).astype(bf16)
        for c in range(cores):
            ts_send[k, c] = y[:, c * share * deep : (c + 1) * share * deep]
        for m in range(1, cores):
            start(sum_copy(k, m))

    def reduce(k):
        total = ts_send[k, core].astype(f32)
        for m in range(1, cores):
            landed(sum_copy(k, m))
            total = total + ts_recv[k, m].astype(f32)
        total = total.astype(bf16)
        for j in range(far):
            rs_send[k, j] = total[j * rows : (j + 1) * rows]
        for j in reversed(range(far - 1)):
            start(reduce_copy(k, j, True))
        rs_recv[z, order[k]] = rs_send[k, z]

    ring_done(far)
    down(0)
    ring_forward(far + 1)
    if far > 2:
        ring_start(far + 2)
    reduce(0)
    for k in range(1, far):
        ring_done(far + k)
        down(k)
        if k + 1 < far:
            ring_forward(far + k + 1)
        if k + 2 < far:
            ring_start(far + k + 2)
        reduce(k)

    mine = []
    for zz in range(far):
        total = None
        for src in range(far):
            landed(
                copy(rs_send.at[0, 0], rs_recv.at[src, zz], rs_s.at[0, 0], rs_r.at[zz, src], at(src, p)),
                z != src,
            )
            one = rs_recv[src, zz].astype(f32)
            total = one if total is None else total + one
        mine.append(total)
    fin_all[core] = jnp.concatenate(mine, axis=1).astype(bf16)

    def final_copy(m, out):
        slot = core if out else (core + cores - m) % cores
        return copy(fin_all.at[slot], fin_all.at[slot], fin_s.at[m], fin_r.at[m], mate(m))

    for m in range(1, cores):
        start(final_copy(m, True))
    for m in range(1, cores):
        landed(final_copy(m, False))
    feed = [fin_all[c].astype(f32) for c in range(cores)]
    whole = jnp.concatenate(
        [
            feed[pp // share][:, (zz * share + pp % share) * deep : (zz * share + pp % share + 1) * deep]
            for zz in range(far)
            for pp in range(near)
        ],
        axis=1,
    )
    parts = [
        alpha_mix * x_all[z, b].astype(f32) + whole[:, b * wide : (b + 1) * wide]
        for b in range(cores)
    ]
    mean = sum(jnp.sum(x, axis=1, keepdims=True) for x in parts) / model
    parts = [x - mean for x in parts]
    var = sum(jnp.sum(x * x, axis=1, keepdims=True) for x in parts) / model
    scale = lax.rsqrt(var + norm_eps)
    for b, x in enumerate(parts):
        xs[b] = x * scale
    out_ref[...] = (xs[core] * cg_ref[...] + cb_ref[...]).astype(bf16)

    for c, when in sends:
        if when is None:
            c.wait_send()
        else:
            pl.when(when)(c.wait_send)


def shards(
    query_logits, value_rows, onward_forget_logits, reverse_forget_logits, output_gate_logits,
    onward_floor_gap, reverse_floor_gap, extra_log_decay, per_head_gain, residual, output_matrix,
    inner_norm_gain, inner_norm_bias, gate_matrix, up_matrix, down_matrix,
    closing_norm_gain, closing_norm_bias,
):
    count, cores = lax.axis_size("sp"), lax.axis_size("tp")
    far = math.gcd(count, 4)
    near = count // far
    rows, span = query_logits.shape
    heads = extra_log_decay.shape[1]
    width = span // heads
    wide = residual.shape[1]
    units = gate_matrix.shape[1] // far
    deep = gate_matrix.shape[0]
    chunk = heads * width // near
    share = near // cores
    n2 = near // 2
    inner_rows = output_matrix.shape[0]
    vm = pltpu.VMEM
    dma = lambda *shape: pltpu.SemaphoreType.DMA(shape)
    scratch = [
        vm((near, far, 2, units, deep), bf16), vm((near, far, units, deep), bf16),
        vm((far, 2, units, deep), bf16),
        vm((near, 2, chunk, width), bf16), vm((near, 2, 1, width), f32),
        vm((near, 2, chunk, width), bf16), vm((near, 2, 1, width), f32),
        vm((2, chunk, width), bf16), vm((2, 1, width), f32),
        vm((2, far, chunk, width), bf16), vm((2, far, 1, width), f32),
        vm((near, 2, chunk, width), bf16), vm((near, 2, chunk, width), bf16),
        vm((cores, inner_rows, wide), bf16), vm((cores, rows, wide), bf16),
        vm((cores, 1, wide), f32), vm((cores, 1, wide), f32),
        vm((cores, rows, span), bf16), vm((far, cores, rows, wide), bf16),
        vm((rows, span), f32), vm((2, rows, span), bf16), vm((far * rows, units), bf16),
        vm((far, cores, far * rows, share * deep), bf16),
        vm((far, cores, far * rows, share * deep), bf16),
        vm((far, far, rows, share * deep), bf16), vm((far, far, rows, share * deep), bf16),
        vm((cores, rows, far * share * deep), bf16), vm((cores, rows, wide), f32),
        dma(2, far), dma(2, far), dma(2, n2, 2 * far), dma(2, n2, 2 * far),
        dma(2, near), dma(2, near), dma(2, 2, far), dma(2, 2, far), dma(near), dma(near),
        dma(4, cores), dma(4, cores), dma(cores), dma(cores), dma(2, far), dma(2, far),
        dma(2, far, cores), dma(2, far, cores), dma(far, cores), dma(far, cores),
        dma(far, far), dma(far, far), dma(cores), dma(cores), dma(1),
    ]
    vmem = pl.BlockSpec(memory_space=pltpu.VMEM)
    specs = [vmem] * 18
    specs[10] = pl.BlockSpec(memory_space=pl.ANY)
    return pl.pallas_call(
        functools.partial(layer_kernel, far, near, cores),
        out_shape=jax.ShapeDtypeStruct((rows, wide), bf16),
        in_specs=specs,
        out_specs=vmem,
        scratch_shapes=scratch,
        compiler_params=pltpu.CompilerParams(
            collective_id=0, has_side_effects=True, vmem_limit_bytes=60 * 1024 * 1024
        ),
    )(
        query_logits, value_rows, onward_forget_logits, reverse_forget_logits, output_gate_logits,
        onward_floor_gap[None], reverse_floor_gap[None], extra_log_decay, per_head_gain[None],
        residual, output_matrix, inner_norm_gain[None], inner_norm_bias[None], gate_matrix,
        up_matrix, down_matrix, closing_norm_gain[None], closing_norm_bias[None],
    )


def solution(mesh):
    a, b = P("sp", "tp"), P("tp")
    placed = (a, a, a, a, a, b, b, a, P(), a, P(None, "tp"), b, b, a, a, P("tp", "sp"), b, b)
    return jax.shard_map(
        shards, mesh=mesh, in_specs=placed, out_specs=P("sp", "tp"), check_vma=False
    )
```

profile of v0, /device:TPU:0, one launch (start us, length us, event | category | flops | bytes accessed | tf_op | source)
XLA Modules:
  0.0 120.0 jit_solution(2315046239718685592)
XLA Ops:
  0.0 1.4 %copy.19.ex_ref = f32[128,4]{1,0:T(8,128)} copy(f32[128,4]{0,1:T(4,128)} %param.25) | data formatting | bytes 4096 | tf_op args[7]
  1.4 116.9 %shard_map.172 = bf16[128,1024]{1,0:T(8,128)(2,1)} custom-call(bf16[128,512]{1,0:T(8,128)(2,1)} %q_ref.1, bf16[128,512]{1,0:T(8,128)(2,1)} %v_ref.1, bf16[128,512]{1,0:T(8,128)(2,1)} %f_ref.1, bf16[128,512]{1,0:T(8,128)(2,1)} %r_ref.1, bf16[128,512]{1,0:T(8,128)(2,1)} %og_ref.1, f32[1,512]{1,0:T(1,128)} %bitcast.11, f32[1,512]{1,0:T(1,128)} %bitcast.12, ...), custom_call_target="tpu_custom_call" | custom-call | tf_op jit(solution)/shard_map/pallas_call | solution.py:545
  118.3 1.7 %copy.21 = bf16[128,1024]{1,0:T(8,128)(2,1)} copy(bf16[128,1024]{1,0:T(8,128)(2,1)} %shard_map.172) | data formatting | bytes 524288
where the time goes:
time: 121 us; the launch traced here: 120 us
  Pallas kernels  117 us (97%)
  local copies, waits for them, and re-layouts  3.09 us (3%)
    pallas_call x1, Pallas kernels, shards(): pl.pallas_call(functools.partial(layer_kernel, far, near, cores), out_sha...  117 us
    unnamed x2, local copies, waits for them, and re-layouts  3.09 us

commit v1 on v0

v1 whole, which is shorter than its diff:
```python
import functools
import math

import jax
import jax.numpy as jnp
from jax import lax
from jax.experimental import pallas as pl
from jax.experimental.pallas import tpu as pltpu
from jax.sharding import PartitionSpec as P

highest = lax.Precision.HIGHEST
alpha_mix = 2.0**0.25
norm_eps = 1e-05
head_eps = 1e-06
bf16 = jnp.bfloat16
f32 = jnp.float32
MESH = pl.DeviceIdType.MESH
pieces = 2


def pick(table, at):
    out = jnp.int32(table[0])
    for i, value in enumerate(table[1:], 1):
        out = jnp.where(at == i, jnp.int32(value), out)
    return out


def across(x, w):
    return lax.dot_general(x, w, (((1,), (1,)), ((), ())), preferred_element_type=f32)


def silu(x):
    return x / (1.0 + jnp.exp(-x))


def layer_kernel(
    far, near, cores,
    q_ref, v_ref, f_ref, r_ref, og_ref, fg_ref, rg_ref, ex_ref, hg_ref, res_ref, om_ref, ig_ref,
    ib_ref, gate_ref, up_ref, down_ref, cg_ref, cb_ref, out_ref,
    wbuf, wsend, st_send, tot_send, st_recv, tot_recv, fs_send, ft_send, f_recv, ft_recv,
    b_send, b_recv, om_all, res_all, ig_all, ib_all, g_all, x_all, inner, dq, hid, ts_send,
    ts_recv, rs_send, rs_recv, fin_all, xs,
    deal_s, deal_r, ring_s, ring_r, half_r, s1_s, s1_r, s2_s, s2_r, s3_s, s3_r, tp_s, tp_r, ga_s, ga_r,
    ag_s, ag_r, d2_s, d2_r, ts_s, ts_r, rs_s, rs_r, fin_s, fin_r, own_s,
):
    rows = q_ref.shape[0]
    heads, width = ex_ref.shape[0], hg_ref.shape[1]
    units, deep = wbuf.shape[3:]
    chunk = st_send.shape[2]
    per_head = near // heads
    share = near // cores
    half = (units // 2 + 15) // 16 * 16
    n2 = near // 2
    me, core = lax.axis_index("sp"), lax.axis_index("tp")
    z, p = me // near, me % near

    ring = [i ^ (i >> 1) for i in range(near)]
    spot = [ring.index(i) for i in range(near)]
    right = pick([ring[(spot[i] + 1) % near] for i in range(near)], p)
    left = pick([ring[(spot[i] - 1) % near] for i in range(near)], p)

    def behind(sign, d):
        return pick([ring[(spot[i] - sign * d) % near] for i in range(near)], p)

    partners = [sorted((j for j in range(far) if j != i), key=lambda j: (abs(j - i), j != i ^ 1))
                for i in range(far)]
    order = [z] + [pick([partners[i][k] for i in range(far)], z) for k in range(far - 1)]

    def copy(src, dst, ssem, rsem, to):
        return pltpu.make_async_remote_copy(
            src_ref=src, dst_ref=dst, send_sem=ssem, recv_sem=rsem, device_id=to,
            device_id_type=MESH,
        )

    def start(c, when=None):
        if when is None:
            c.start()
        else:
            pl.when(when)(c.start)

    def sent(sem, ref):
        copy(ref, ref, sem, sem, mate(1)).wait_send()

    def came(sem, ref):
        copy(ref, ref, sem, sem, mate(1)).wait_recv()

    def landed(c, when=None):
        if when is None:
            c.wait_recv()
        else:
            pl.when(when)(c.wait_recv)

    def at(zz, pp):
        return (zz * near + pp, core)

    def mate(m):
        return (me, (core + m) % cores)

    f_recv[...] = jnp.zeros_like(f_recv)
    ft_recv[...] = jnp.zeros_like(ft_recv)

    barrier = pltpu.get_barrier_semaphore()
    peers = [at(z, (p + j) % near) for j in range(1, near)]
    peers += [at((z + j) % far, p) for j in range(1, far)]
    peers += [mate(m) for m in range(1, cores)]
    for peer in peers:
        pl.semaphore_signal(barrier, inc=1, device_id=peer, device_id_type=MESH)

    own_om = pltpu.make_async_copy(om_ref, om_all.at[core], own_s.at[0])
    own_om.start()
    for i, ref in enumerate((gate_ref, up_ref)):
        whole = ref[...].astype(f32).T
        for j in range(far):
            wsend[j, i] = whole[j * units : (j + 1) * units].astype(bf16)
    wbuf[p, z, 0] = wsend[z, 0]
    wbuf[p, z, 1] = wsend[z, 1]
    wbuf[p, z, 2] = down_ref[pl.ds(pl.multiple_of(z * units, 16), units), :]
    res_all[core] = res_ref[...]
    ig_all[core] = ig_ref[...]
    ib_all[core] = ib_ref[...]
    pl.semaphore_wait(barrier, len(peers))

    def deal_copy(g, peer, slot, e):
        if g < 2:
            src = wsend.at[peer, g]
        else:
            src = down_ref.at[pl.ds(pl.multiple_of(peer * units, 16), units), :]
        return copy(src, wbuf.at[p, slot, g], deal_s.at[0], deal_r.at[g, slot], at(peer, p))

    def deal(g, e):
        start(deal_copy(g, (z + e) % far, z, e), z + e < far)
        start(deal_copy(g, (z + far - e) % far, z, far + e), z >= e)

    def ring_copy(k, sign, d, block):
        side = 0 if sign > 0 else 1
        ref = wbuf.at[block, order[k % far], k // far]
        if d == n2:
            ref = ref.at[pl.ds(0, half), :] if side == 0 else ref.at[pl.ds(half, units - half), :]
        to = right if sign > 0 else left
        if d < n2:
            arrive = ring_r.at[side, d - 1, k]
        else:
            arrive = half_r.at[max(0, k - 2 * far + 1)]
        return copy(ref, ref, ring_s.at[0], arrive, at(z, to))

    def ring_start(k):
        if k % far:
            landed(deal_copy(k // far, order[k % far], order[k % far], 0))
        for sign in (1, -1):
            start(ring_copy(k, sign, 1, p))

    def ring_forward(k):
        for d in range(1, n2):
            for sign in (1, -1):
                block = behind(sign, d)
                landed(ring_copy(k, sign, d, block))
                start(ring_copy(k, sign, d + 1, block))

    def ring_done(k):
        came(half_r.at[k - 2 * far + 1], wbuf.at[0, 0, 2])

    g0, u0, d0 = 0, far, 2 * far
    for g in range(2):
        deal(g, 1)
    ring_start(g0)

    pairs = ((om_ref, om_all), (res_ref, res_all), (ig_ref, ig_all), (ib_ref, ib_all))

    def tp_copy(i, m):
        src, dst = pairs[i]
        return copy(src, dst.at[core], tp_s.at[i], tp_r.at[i], mate(m))

    for m in range(1, cores):
        for i in range(len(pairs)):
            start(tp_copy(i, m))


    t = lax.broadcasted_iota(jnp.int32, (rows, rows), 0)
    s = lax.broadcasted_iota(jnp.int32, (rows, rows), 1)
    lower, upper = s <= t, s >= t
    for h in range(heads):
        cols = slice(h * width, (h + 1) * width)
        q = silu(q_ref[:, cols].astype(f32))
        v = v_ref[:, cols]
        extra = jnp.broadcast_to(ex_ref[h : h + 1, :], (width, rows)).T
        scores = jnp.zeros((rows, rows), f32)
        for d, (raw_ref, gap_ref, tri) in enumerate(
            ((f_ref, fg_ref, lower), (r_ref, rg_ref, upper))
        ):
            raw = raw_ref[:, cols].astype(f32)
            key = gap_ref[:, cols] * (1.0 / (1.0 + jnp.exp(raw)))
            log = jnp.log1p(-key) + extra
            run = jnp.dot(tri.astype(f32), log, precision=highest, preferred_element_type=f32)
            last = run[rows - 1 :, :] if d == 0 else run[:1, :]
            qd = (q * jnp.exp(run)).astype(bf16)
            ki = (key * jnp.exp(-run)).astype(bf16)
            ks = (key * jnp.exp(last - run)).astype(bf16)
            scores = scores + jnp.where(tri, across(qd, ki), 0.0)
            dq[d, :, cols] = qd
            state = lax.dot_general(v, ks, (((0,), (0,)), ((), ())), preferred_element_type=f32)
            for i in range(per_head):
                st_send[h * per_head + i, d] = state[i * chunk : (i + 1) * chunk].astype(bf16)
                tot_send[h * per_head + i, d] = last
        inner[:, cols] = jnp.dot(scores.astype(bf16), v, preferred_element_type=f32)

    def plane_copy(i, j):
        src, dst = ((st_send, st_recv), (tot_send, tot_recv))[i]
        to = (p + j) % near
        return copy(src.at[to], dst.at[p], s1_s.at[i], s1_r.at[i], at(z, to))

    for j in range(1, near):
        for i in range(2):
            start(plane_copy(i, j))
    st_recv[p] = st_send[p]
    tot_recv[p] = tot_send[p]

    came(s1_r.at[0], st_recv.at[pl.ds(0, near - 1)])
    came(s1_r.at[1], tot_recv.at[pl.ds(0, near - 1)])

    prefix = [[None] * near, [None] * near]
    gone = [[None] * near, [None] * near]
    for d in range(2):
        state = jnp.zeros((chunk, width), f32)
        total = jnp.zeros((1, width), f32)
        for b in range(near) if d == 0 else reversed(range(near)):
            prefix[d][b], gone[d][b] = state, total
            step = tot_recv[b, d]
            state = state * jnp.exp(step) + st_recv[b, d].astype(f32)
            total = total + step
        fs_send[d] = state.astype(bf16)
        ft_send[d] = total

    def far_copy(i, d, e):
        src, dst = ((fs_send, f_recv), (ft_send, ft_recv))[i]
        to = (z + e) % far if d == 0 else (z + far - e) % far
        return copy(src.at[d], dst.at[d, e], s2_s.at[i], s2_r.at[i], at(to, p))

    def far_valid(d, e):
        return z + e < far if d == 0 else z >= e

    for e in range(1, far):
        for d in range(2):
            for i in range(2):
                start(far_copy(i, d, e), far_valid(d, e))

    ring_start(u0)

    came(s2_r.at[0], f_recv.at[0, pl.ds(1, far - 1)])
    came(s2_r.at[1], ft_recv.at[0, pl.ds(1, far - 1)])

    for d in range(2):
        enter = jnp.zeros((chunk, width), f32)
        for e in reversed(range(1, far)):
            enter = enter * jnp.exp(ft_recv[d, e]) + f_recv[d, e].astype(f32)
        for b in range(near):
            b_send[b, d] = (enter * jnp.exp(gone[d][b]) + prefix[d][b]).astype(bf16)

    def back_copy(j):
        to = (p + j) % near
        return copy(b_send.at[to], b_recv.at[p], s3_s.at[0], s3_r.at[0], at(z, to))

    for j in range(1, near):
        start(back_copy(j))
    b_recv[p] = b_send[p]

    deal(0, 2)
    deal(1, 2)
    ring_forward(g0)
    ring_start(g0 + 1)

    came(s3_r.at[0], b_recv.at[pl.ds(0, near - 1)])

    for h in range(heads):
        cols = slice(h * width, (h + 1) * width)
        mixed = inner[:, cols]
        for d in range(2):
            state = jnp.concatenate(
                [b_recv[h * per_head + i, d].astype(f32) for i in range(per_head)], axis=0
            ).astype(bf16)
            mixed = mixed + across(dq[d, :, cols], state)
        normed = (
            mixed
            * lax.rsqrt(jnp.mean(mixed * mixed, axis=1, keepdims=True) + head_eps)
            * hg_ref[...]
        )
        g_all[core, :, cols] = (normed * silu(og_ref[:, cols].astype(f32))).astype(bf16)

    for m in range(1, cores):
        start(copy(g_all.at[core], g_all.at[core], ga_s.at[0], ga_r.at[0], mate(m)))
    ring_forward(u0)
    ring_start(u0 + 1)
    own_om.wait()
    for i in range(len(pairs)):
        came(tp_r.at[i], pairs[i][1].at[pl.ds(0, cores - 1)])
    came(ga_r.at[0], g_all.at[pl.ds(0, cores - 1)])

    span = q_ref.shape[1]
    parts = []
    for b in range(cores):
        mixer = alpha_mix * res_all[b].astype(f32)
        for m in range(cores):
            mixer = mixer + jnp.dot(
                g_all[m], om_all[b, m * span : (m + 1) * span, :], preferred_element_type=f32
            )
        parts.append(mixer)
    wide = parts[0].shape[1]
    model = cores * wide
    mean = sum(jnp.sum(x, axis=1, keepdims=True) for x in parts) / model
    parts = [x - mean for x in parts]
    var = sum(jnp.sum(x * x, axis=1, keepdims=True) for x in parts) / model
    scale = lax.rsqrt(var + norm_eps)
    for b, x in enumerate(parts):
        x_all[z, b] = (x * scale * ig_all[b] + ib_all[b]).astype(bf16)

    part = rows // pieces

    def line_copy(sign, d, i, out):
        block = (z + far + ((1 if out else 0) - d) * sign) % far
        side = 0 if sign > 0 else 1
        ref = x_all.at[block, core, pl.ds(i * part, part), :]
        to = at((z + far + sign) % far, p)
        return copy(ref, ref, ag_s.at[side, d - 1, i], ag_r.at[side, d - 1, i], to)

    def line_out(sign, d):
        if sign > 0:
            return jnp.logical_and(z + 1 < far, z >= d - 1)
        return jnp.logical_and(z > 0, z + d - 1 < far)

    def line_in(sign, d):
        return z >= d if sign > 0 else z + d < far

    def line_share(sign, d, i, m):
        ref = x_all.at[(z + far - d * sign) % far, core, pl.ds(i * part, part), :]
        return copy(ref, ref, d2_s.at[0], d2_r.at[0], mate(m))

    def line_step(d, i):
        for sign in (1, -1):
            landed(line_copy(sign, d, i, False), line_in(sign, d))
            if d + 1 < far:
                start(line_copy(sign, d + 1, i, True), line_out(sign, d + 1))
            for m in range(1, cores):
                start(line_share(sign, d, i, m), line_in(sign, d))

    for i in range(pieces):
        for sign in (1, -1):
            start(line_copy(sign, 1, i, True), line_out(sign, 1))
    deal(0, 3)
    ring_start(g0 + 2)
    ring_forward(g0 + 1)
    ring_forward(u0 + 1)
    ring_start(u0 + 2)
    ring_forward(g0 + 2)
    for i in range(pieces):
        line_step(1, i)
    deal(1, 3)
    ring_start(g0 + 3)
    line_step(2, 0)
    deal(2, 1)
    ring_forward(u0 + 2)
    for i in range(1, pieces):
        line_step(2, i)
    ring_start(u0 + 3)
    ring_forward(g0 + 3)
    ring_start(d0)
    for i in range(pieces):
        line_step(3, i)
    deal(2, 2)
    deal(2, 3)
    ring_forward(u0 + 3)
    ring_forward(d0)
    ring_start(d0 + 1)
    came(d2_r.at[0], x_all.at[pl.ds(0, far - 1), pl.ds(0, cores - 1)])
    came(half_r.at[0], wbuf.at[0, :, pl.ds(0, 2)])

    step = 256
    for n0 in range(0, units, step):
        n1 = min(units, n0 + step)
        gate = up = 0.0
        for pp in range(near):
            spots = [(zz * near + pp) * deep for zz in range(far)]
            x = jnp.concatenate(
                [
                    jnp.concatenate(
                        [x_all[j, c // wide, :, c % wide : c % wide + deep] for c in spots], axis=1
                    )
                    for j in range(far)
                ],
                axis=0,
            )
            wg, wu = (
                jnp.concatenate([wbuf[pp, zz, i, n0:n1, :] for zz in range(far)], axis=1)
                for i in range(2)
            )
            gate = gate + across(x, wg)
            up = up + across(x, wu)
        hid[:, n0:n1] = (silu(gate) * up).astype(bf16)

    def sum_copy(k, m):
        return copy(
            ts_send.at[k, (core + m) % cores], ts_recv.at[k, m - 1], ts_s.at[0], ts_r.at[k],
            mate(m),
        )

    def reduce_copy(k, j):
        to = order[j + 1]
        return copy(
            rs_send.at[k, to], rs_recv.at[z, order[k]], rs_s.at[0], rs_r.at[0], at(to, p)
        )

    def down(k):
        zz = order[k]
        w = jnp.concatenate([wbuf[pp, zz, 2] for pp in range(near)], axis=1)
        y = jnp.dot(hid[...], w, preferred_element_type=f32).astype(bf16)
        for c in range(cores):
            ts_send[k, c] = y[:, c * share * deep : (c + 1) * share * deep]
        for m in range(1, cores):
            start(sum_copy(k, m))

    def reduce(k):
        total = ts_send[k, core].astype(f32)
        came(ts_r.at[k], ts_recv.at[k])
        for m in range(1, cores):
            total = total + ts_recv[k, m - 1].astype(f32)
        total = total.astype(bf16)
        for j in range(far):
            rs_send[k, j] = total[j * rows : (j + 1) * rows]
        for j in reversed(range(far - 1)):
            start(reduce_copy(k, j))
        rs_recv[z, order[k]] = rs_send[k, z]

    ring_start(d0 + 2)
    for k in range(far):
        ring_done(d0 + k)
        down(k)
        if k + 1 < far:
            ring_forward(d0 + k + 1)
        if k + 3 < far:
            ring_start(d0 + k + 3)
        reduce(k)

    came(rs_r.at[0], rs_recv.at[pl.ds(0, far - 1)])
    mine = [sum(rs_recv[src, zz].astype(f32) for src in range(far)) for zz in range(far)]
    fin_all[core] = jnp.concatenate(mine, axis=1).astype(bf16)

    for m in range(1, cores):
        start(copy(fin_all.at[core], fin_all.at[core], fin_s.at[0], fin_r.at[0], mate(m)))
    came(fin_r.at[0], fin_all.at[pl.ds(0, cores - 1)])
    feed = [fin_all[c].astype(f32) for c in range(cores)]
    whole = jnp.concatenate(
        [
            feed[pp // share][:, (zz * share + pp % share) * deep : (zz * share + pp % share + 1) * deep]
            for zz in range(far)
            for pp in range(near)
        ],
        axis=1,
    )
    parts = [
        alpha_mix * x_all[z, b].astype(f32) + whole[:, b * wide : (b + 1) * wide]
        for b in range(cores)
    ]
    mean = sum(jnp.sum(x, axis=1, keepdims=True) for x in parts) / model
    parts = [x - mean for x in parts]
    var = sum(jnp.sum(x * x, axis=1, keepdims=True) for x in parts) / model
    scale = lax.rsqrt(var + norm_eps)
    for b, x in enumerate(parts):
        xs[b] = x * scale
    out_ref[...] = (xs[core] * cg_ref[...] + cb_ref[...]).astype(bf16)

    sent(deal_s.at[0], wbuf.at[0, pl.ds(0, far - 1)])
    sent(ring_s.at[0], wbuf.at[pl.ds(0, near - 1)])
    for i in range(len(pairs)):
        sent(tp_s.at[i], pairs[i][1].at[pl.ds(0, cores - 1)])
    sent(s1_s.at[0], st_recv.at[pl.ds(0, near - 1)])
    sent(s1_s.at[1], tot_recv.at[pl.ds(0, near - 1)])
    sent(s2_s.at[0], f_recv.at[0, pl.ds(1, far - 1)])
    sent(s2_s.at[1], ft_recv.at[0, pl.ds(1, far - 1)])
    sent(s3_s.at[0], b_recv.at[pl.ds(0, near - 1)])
    sent(ga_s.at[0], g_all.at[pl.ds(0, cores - 1)])
    for d in range(1, far):
        for sign in (1, -1):
            for i in range(pieces):
                pl.when(line_out(sign, d))(line_copy(sign, d, i, True).wait_send)
    sent(d2_s.at[0], x_all.at[pl.ds(0, far - 1), pl.ds(0, cores - 1)])
    sent(ts_s.at[0], ts_recv)
    sent(rs_s.at[0], rs_recv.at[pl.ds(0, far - 1)])
    sent(fin_s.at[0], fin_all.at[pl.ds(0, cores - 1)])


def shards(
    query_logits, value_rows, onward_forget_logits, reverse_forget_logits, output_gate_logits,
    onward_floor_gap, reverse_floor_gap, extra_log_decay, per_head_gain, residual, output_matrix,
    inner_norm_gain, inner_norm_bias, gate_matrix, up_matrix, down_matrix,
    closing_norm_gain, closing_norm_bias,
):
    count, cores = lax.axis_size("sp"), lax.axis_size("tp")
    far = math.gcd(count, 4)
    near = count // far
    rows, span = query_logits.shape
    heads = extra_log_decay.shape[1]
    width = span // heads
    wide = residual.shape[1]
    units = gate_matrix.shape[1] // far
    deep = gate_matrix.shape[0]
    chunk = heads * width // near
    share = near // cores
    n2 = near // 2
    inner_rows = output_matrix.shape[0]
    vm = pltpu.VMEM
    dma = lambda *shape: pltpu.SemaphoreType.DMA(shape)
    scratch = [
        vm((near, far, 3, units, deep), bf16),
        vm((far, 2, units, deep), bf16),
        vm((near, 2, chunk, width), bf16), vm((near, 2, 1, width), f32),
        vm((near, 2, chunk, width), bf16), vm((near, 2, 1, width), f32),
        vm((2, chunk, width), bf16), vm((2, 1, width), f32),
        vm((2, far, chunk, width), bf16), vm((2, far, 1, width), f32),
        vm((near, 2, chunk, width), bf16), vm((near, 2, chunk, width), bf16),
        vm((cores, inner_rows, wide), bf16), vm((cores, rows, wide), bf16),
        vm((cores, 1, wide), f32), vm((cores, 1, wide), f32),
        vm((cores, rows, span), bf16), vm((far, cores, rows, wide), bf16),
        vm((rows, span), f32), vm((2, rows, span), bf16), vm((far * rows, units), bf16),
        vm((far, cores, far * rows, share * deep), bf16),
        vm((far, cores - 1, far * rows, share * deep), bf16),
        vm((far, far, rows, share * deep), bf16), vm((far, far, rows, share * deep), bf16),
        vm((cores, rows, far * share * deep), bf16), vm((cores, rows, wide), f32),
        dma(1), dma(3, far), dma(1), dma(2, n2 - 1, 3 * far), dma(far + 1),
        dma(2), dma(2), dma(2), dma(2), dma(1), dma(1), dma(4), dma(4), dma(1), dma(1),
        dma(2, far - 1, pieces), dma(2, far - 1, pieces), dma(1), dma(1), dma(1), dma(far),
        dma(1), dma(1), dma(1), dma(1), dma(1),
    ]
    vmem = pl.BlockSpec(memory_space=pltpu.VMEM)
    specs = [vmem] * 18
    specs[10] = pl.BlockSpec(memory_space=pl.ANY)
    return pl.pallas_call(
        functools.partial(layer_kernel, far, near, cores),
        out_shape=jax.ShapeDtypeStruct((rows, wide), bf16),
        in_specs=specs,
        out_specs=vmem,
        scratch_shapes=scratch,
        compiler_params=pltpu.CompilerParams(
            collective_id=0, has_side_effects=True, vmem_limit_bytes=60 * 1024 * 1024
        ),
    )(
        query_logits, value_rows, onward_forget_logits, reverse_forget_logits, output_gate_logits,
        onward_floor_gap[None], reverse_floor_gap[None], extra_log_decay.T, per_head_gain[None],
        residual, output_matrix, inner_norm_gain[None], inner_norm_bias[None], gate_matrix,
        up_matrix, down_matrix, closing_norm_gain[None], closing_norm_bias[None],
    )


def solution(mesh):
    a, b = P("sp", "tp"), P("tp")
    placed = (a, a, a, a, a, b, b, a, P(), a, P(None, "tp"), b, b, a, a, P("tp", "sp"), b, b)
    return jax.shard_map(
        shards, mesh=mesh, in_specs=placed, out_specs=P("sp", "tp"), check_vma=False
    )
```

time: 121 us -> 106 us (0.88)
  Pallas kernels: 117 us -> 104 us
  local copies, waits for them, and re-layouts: 3.09 us -> 1.67 us
    pallas_call x1, Pallas kernels: 117 us -> 104 us  [shards(): pl.pallas_call(functools.partial(layer_kernel, far, near, cores), out_sha...]
    unnamed x2 -> x1, local copies, waits for them, and re-layouts: 3.09 us -> 1.67 us
where the time goes in v1:
time: 106 us; the launch traced here: 105 us
  Pallas kernels  104 us (98%)
  local copies, waits for them, and re-layouts  1.67 us (2%)
    pallas_call x1, Pallas kernels, shards(): pl.pallas_call(functools.partial(layer_kernel, far, near, cores), out_sha...  104 us

profile of v1, /device:TPU:0, one launch (start us, length us, event | category | flops | bytes accessed | tf_op | source)
XLA Modules:
  0.0 105.3 jit_solution(3190340121355153856)
XLA Ops:
  0.0 103.6 %shard_map.172 = bf16[128,1024]{1,0:T(8,128)(2,1)} custom-call(bf16[128,512]{1,0:T(8,128)(2,1)} %q_ref.1, bf16[128,512]{1,0:T(8,128)(2,1)} %v_ref.1, bf16[128,512]{1,0:T(8,128)(2,1)} %f_ref.1, bf16[128,512]{1,0:T(8,128)(2,1)} %r_ref.1, bf16[128,512]{1,0:T(8,128)(2,1)} %og_ref.1, f32[1,512]{1,0:T(1,128)} %bitcast.12, f32[1,512]{1,0:T(1,128)} %bitcast.13, ...), custom_call_target="tpu_custom_call" | custom-call | tf_op jit(solution)/shard_map/pallas_call | solution.py:534
  103.6 1.7 %copy.20 = bf16[128,1024]{1,0:T(8,128)(2,1)} copy(bf16[128,1024]{1,0:T(8,128)(2,1)} %shard_map.172) | data formatting | bytes 524288

commit v2 on v1

--- a/solution.py
+++ b/solution.py
@@ -35,16 +35,18 @@
 
 def layer_kernel(
     far, near, cores,
-    q_ref, v_ref, f_ref, r_ref, og_ref, fg_ref, rg_ref, ex_ref, hg_ref, res_ref, om_ref, ig_ref,
-    ib_ref, gate_ref, up_ref, down_ref, cg_ref, cb_ref, out_ref,
+    q_in, v_in, f_in, r_in, og_in, fg_in, rg_in, ex_in, hg_in, res_ref, om_ref, ig_ref, ib_ref,
+    gate_in, up_in, down_ref, cg_in, cb_in, out_ref,
+    q_ref, v_ref, f_ref, r_ref, og_ref, fg_ref, rg_ref, ex_ref, hg_ref, gate_ref, up_ref, cg_ref,
+    cb_ref,
     wbuf, wsend, st_send, tot_send, st_recv, tot_recv, fs_send, ft_send, f_recv, ft_recv,
     b_send, b_recv, om_all, res_all, ig_all, ib_all, g_all, x_all, inner, dq, hid, ts_send,
     ts_recv, rs_send, rs_recv, fin_all, xs,
     deal_s, deal_r, ring_s, ring_r, half_r, s1_s, s1_r, s2_s, s2_r, s3_s, s3_r, tp_s, tp_r, ga_s, ga_r,
-    ag_s, ag_r, d2_s, d2_r, ts_s, ts_r, rs_s, rs_r, fin_s, fin_r, own_s,
+    ag_s, ag_r, d2_s, d2_r, ts_s, ts_r, rs_s, rs_r, fin_s, fin_r, load_s,
 ):
-    rows = q_ref.shape[0]
-    heads, width = ex_ref.shape[0], hg_ref.shape[1]
+    rows = q_in.shape[0]
+    heads, width = ex_in.shape[0], hg_in.shape[1]
     units, deep = wbuf.shape[3:]
     chunk = st_send.shape[2]
     per_head = near // heads
@@ -96,6 +98,22 @@
     def mate(m):
         return (me, (core + m) % cores)
 
+    down_own = down_ref.at[pl.ds(pl.multiple_of(z * units, 16), units), :]
+    loads = {}
+    for name, src, dst in (
+        ("gate", gate_in, gate_ref), ("up", up_in, up_ref), ("f", f_in, f_ref),
+        ("r", r_in, r_ref), ("fg", fg_in, fg_ref), ("rg", rg_in, rg_ref), ("ex", ex_in, ex_ref),
+        ("q", q_in, q_ref), ("v", v_in, v_ref), ("down", down_own, wbuf.at[p, z, 2]),
+        ("om", om_ref, om_all.at[core]), ("res", res_ref, res_all.at[core]),
+        ("ig", ig_ref, ig_all.at[core]), ("ib", ib_ref, ib_all.at[core]), ("og", og_in, og_ref),
+        ("hg", hg_in, hg_ref), ("cg", cg_in, cg_ref), ("cb", cb_in, cb_ref),
+    ):
+        loads[name] = pltpu.make_async_copy(src, dst, load_s.at[len(loads)])
+
+    def loaded(*names):
+        for name in names:
+            loads[name].wait()
+
     f_recv[...] = jnp.zeros_like(f_recv)
     ft_recv[...] = jnp.zeros_like(ft_recv)
 
@@ -106,18 +124,15 @@
     for peer in peers:
         pl.semaphore_signal(barrier, inc=1, device_id=peer, device_id_type=MESH)
 
-    own_om = pltpu.make_async_copy(om_ref, om_all.at[core], own_s.at[0])
-    own_om.start()
+    for load in loads.values():
+        load.start()
+    loaded("gate", "up")
     for i, ref in enumerate((gate_ref, up_ref)):
         whole = ref[...].astype(f32).T
         for j in range(far):
             wsend[j, i] = whole[j * units : (j + 1) * units].astype(bf16)
     wbuf[p, z, 0] = wsend[z, 0]
     wbuf[p, z, 1] = wsend[z, 1]
-    wbuf[p, z, 2] = down_ref[pl.ds(pl.multiple_of(z * units, 16), units), :]
-    res_all[core] = res_ref[...]
-    ig_all[core] = ig_ref[...]
-    ib_all[core] = ib_ref[...]
     pl.semaphore_wait(barrier, len(peers))
 
     def deal_copy(g, peer, slot, e):
@@ -175,6 +190,7 @@
             start(tp_copy(i, m))
 
 
+    loaded("f", "r", "fg", "rg", "ex", "q", "v")
     t = lax.broadcasted_iota(jnp.int32, (rows, rows), 0)
     s = lax.broadcasted_iota(jnp.int32, (rows, rows), 1)
     lower, upper = s <= t, s >= t
@@ -270,6 +286,7 @@
 
     came(s3_r.at[0], b_recv.at[pl.ds(0, near - 1)])
 
+    loaded("og", "hg")
     for h in range(heads):
         cols = slice(h * width, (h + 1) * width)
         mixed = inner[:, cols]
@@ -289,7 +306,7 @@
         start(copy(g_all.at[core], g_all.at[core], ga_s.at[0], ga_r.at[0], mate(m)))
     ring_forward(u0)
     ring_start(u0 + 1)
-    own_om.wait()
+    loaded("om", "res", "ig", "ib")
     for i in range(len(pairs)):
         came(tp_r.at[i], pairs[i][1].at[pl.ds(0, cores - 1)])
     came(ga_r.at[0], g_all.at[pl.ds(0, cores - 1)])
@@ -355,19 +372,19 @@
     deal(1, 3)
     ring_start(g0 + 3)
     line_step(2, 0)
-    deal(2, 1)
     ring_forward(u0 + 2)
     for i in range(1, pieces):
         line_step(2, i)
+    deal(2, 1)
     ring_start(u0 + 3)
     ring_forward(g0 + 3)
+    ring_forward(u0 + 3)
+    loaded("down")
     ring_start(d0)
     for i in range(pieces):
         line_step(3, i)
     deal(2, 2)
     deal(2, 3)
-    ring_forward(u0 + 3)
-    ring_forward(d0)
     ring_start(d0 + 1)
     came(d2_r.at[0], x_all.at[pl.ds(0, far - 1), pl.ds(0, cores - 1)])
     came(half_r.at[0], wbuf.at[0, :, pl.ds(0, 2)])
@@ -395,56 +412,72 @@
             up = up + across(x, wu)
         hid[:, n0:n1] = (silu(gate) * up).astype(bf16)
 
-    def sum_copy(k, m):
-        return copy(
-            ts_send.at[k, (core + m) % cores], ts_recv.at[k, m - 1], ts_s.at[0], ts_r.at[k],
-            mate(m),
-        )
-
-    def reduce_copy(k, j):
+    close = [p] + [behind(sign, d) for d in range(1, n2) for sign in (1, -1)]
+    opposite = behind(1, n2)
+
+    def sum_copy(k, pp):
+        owner = pp // share
+        dst = ts_recv.at[k, pp % share, (owner + cores - 1 - core) % cores]
+        return copy(ts_send.at[k, pp], dst, ts_s.at[0], ts_r.at[k, pp % share], (me, owner))
+
+    def down(k, slots):
+        w = jnp.concatenate([wbuf[pp, order[k], 2] for pp in slots], axis=1)
+        y = jnp.dot(hid[...], w, preferred_element_type=f32).astype(bf16)
+        for i, pp in enumerate(slots):
+            ts_send[k, pp] = y[:, i * deep : (i + 1) * deep]
+        for pp in slots:
+            start(sum_copy(k, pp), pp // share != core)
+
+    def reduce_copy(k, i, j):
         to = order[j + 1]
-        return copy(
-            rs_send.at[k, to], rs_recv.at[z, order[k]], rs_s.at[0], rs_r.at[0], at(to, p)
-        )
-
-    def down(k):
-        zz = order[k]
-        w = jnp.concatenate([wbuf[pp, zz, 2] for pp in range(near)], axis=1)
-        y = jnp.dot(hid[...], w, preferred_element_type=f32).astype(bf16)
-        for c in range(cores):
-            ts_send[k, c] = y[:, c * share * deep : (c + 1) * share * deep]
-        for m in range(1, cores):
-            start(sum_copy(k, m))
-
-    def reduce(k):
-        total = ts_send[k, core].astype(f32)
-        came(ts_r.at[k], ts_recv.at[k])
-        for m in range(1, cores):
-            total = total + ts_recv[k, m - 1].astype(f32)
+        dst = rs_recv.at[z, order[k], i]
+        return copy(rs_send.at[k, i, to], dst, rs_s.at[0], rs_r.at[0], at(to, p))
+
+    def reduce_slot(k, i):
+        total = ts_send[k, core * share + i].astype(f32)
+        came(ts_r.at[k, i], ts_recv.at[k, i])
+        for m in range(cores - 1):
+            total = total + ts_recv[k, i, m].astype(f32)
         total = total.astype(bf16)
         for j in range(far):
-            rs_send[k, j] = total[j * rows : (j + 1) * rows]
+            rs_send[k, i, j] = total[j * rows : (j + 1) * rows]
         for j in reversed(range(far - 1)):
-            start(reduce_copy(k, j))
-        rs_recv[z, order[k]] = rs_send[k, z]
-
-    ring_start(d0 + 2)
+            start(reduce_copy(k, i, j))
+        rs_recv[z, order[k], i] = rs_send[k, i, z]
+
+    def reduce(k, late):
+        for i in range(share):
+            mine_late = core * share + i == opposite
+            when = mine_late if late else jnp.logical_not(mine_late)
+            pl.when(when)(functools.partial(reduce_slot, k, i))
+
     for k in range(far):
-        ring_done(d0 + k)
-        down(k)
-        if k + 1 < far:
-            ring_forward(d0 + k + 1)
-        if k + 3 < far:
-            ring_start(d0 + k + 3)
-        reduce(k)
+        ring_forward(d0 + k)
+        down(k, close)
+        if k:
+            ring_done(d0 + k - 1)
+            down(k - 1, [opposite])
+        reduce(k, False)
+        if k:
+            reduce(k - 1, True)
+        if k + 2 < far:
+            ring_start(d0 + k + 2)
+    ring_done(d0 + far - 1)
+    down(far - 1, [opposite])
+    reduce(far - 1, True)
 
     came(rs_r.at[0], rs_recv.at[pl.ds(0, far - 1)])
-    mine = [sum(rs_recv[src, zz].astype(f32) for src in range(far)) for zz in range(far)]
+    mine = [
+        sum(rs_recv[src, zz, i].astype(f32) for src in range(far))
+        for zz in range(far)
+        for i in range(share)
+    ]
     fin_all[core] = jnp.concatenate(mine, axis=1).astype(bf16)
 
     for m in range(1, cores):
         start(copy(fin_all.at[core], fin_all.at[core], fin_s.at[0], fin_r.at[0], mate(m)))
     came(fin_r.at[0], fin_all.at[pl.ds(0, cores - 1)])
+    loaded("cg", "cb")
     feed = [fin_all[c].astype(f32) for c in range(cores)]
     whole = jnp.concatenate(
         [
@@ -481,8 +514,8 @@
             for i in range(pieces):
                 pl.when(line_out(sign, d))(line_copy(sign, d, i, True).wait_send)
     sent(d2_s.at[0], x_all.at[pl.ds(0, far - 1), pl.ds(0, cores - 1)])
-    sent(ts_s.at[0], ts_recv)
-    sent(rs_s.at[0], rs_recv.at[pl.ds(0, far - 1)])
+    sent(ts_s.at[0], ts_send.at[:, pl.ds(0, near - share)])
+    sent(rs_s.at[0], rs_send.at[:, :, pl.ds(0, far - 1)])
     sent(fin_s.at[0], fin_all.at[pl.ds(0, cores - 1)])
 
 
@@ -508,6 +541,10 @@
     vm = pltpu.VMEM
     dma = lambda *shape: pltpu.SemaphoreType.DMA(shape)
     scratch = [
+        vm((rows, span), bf16), vm((rows, span), bf16), vm((rows, span), bf16),
+        vm((rows, span), bf16), vm((rows, span), bf16), vm((1, span), f32), vm((1, span), f32),
+        vm((heads, rows), f32), vm((1, width), f32), vm(gate_matrix.shape, bf16),
+        vm(gate_matrix.shape, bf16), vm((1, wide), f32), vm((1, wide), f32),
         vm((near, far, 3, units, deep), bf16),
         vm((far, 2, units, deep), bf16),
         vm((near, 2, chunk, width), bf16), vm((near, 2, 1, width), f32),
@@ -519,18 +556,16 @@
         vm((cores, 1, wide), f32), vm((cores, 1, wide), f32),
         vm((cores, rows, span), bf16), vm((far, cores, rows, wide), bf16),
         vm((rows, span), f32), vm((2, rows, span), bf16), vm((far * rows, units), bf16),
-        vm((far, cores, far * rows, share * deep), bf16),
-        vm((far, cores - 1, far * rows, share * deep), bf16),
-        vm((far, far, rows, share * deep), bf16), vm((far, far, rows, share * deep), bf16),
+        vm((far, near, far * rows, deep), bf16), vm((far, share, cores - 1, far * rows, deep), bf16),
+        vm((far, share, far, rows, deep), bf16), vm((far, far, share, rows, deep), bf16),
         vm((cores, rows, far * share * deep), bf16), vm((cores, rows, wide), f32),
         dma(1), dma(3, far), dma(1), dma(2, n2 - 1, 3 * far), dma(far + 1),
         dma(2), dma(2), dma(2), dma(2), dma(1), dma(1), dma(4), dma(4), dma(1), dma(1),
-        dma(2, far - 1, pieces), dma(2, far - 1, pieces), dma(1), dma(1), dma(1), dma(far),
-        dma(1), dma(1), dma(1), dma(1), dma(1),
+        dma(2, far - 1, pieces), dma(2, far - 1, pieces), dma(1), dma(1), dma(1), dma(far, share),
+        dma(1), dma(1), dma(1), dma(1), dma(18),
     ]
     vmem = pl.BlockSpec(memory_space=pltpu.VMEM)
-    specs = [vmem] * 18
-    specs[10] = pl.BlockSpec(memory_space=pl.ANY)
+    specs = [pl.BlockSpec(memory_space=pl.ANY)] * 18
     return pl.pallas_call(
         functools.partial(layer_kernel, far, near, cores),
         out_shape=jax.ShapeDtypeStruct((rows, wide), bf16),

time: 106 us -> 99.2 us (0.936)
  Pallas kernels: 104 us -> 97.3 us
    pallas_call x1, Pallas kernels: 104 us -> 97.3 us  [shards(): pl.pallas_call(functools.partial(layer_kernel, far, near, cores), out_sha...]
where the time goes in v2:
time: 99.2 us; the launch traced here: 99 us
  Pallas kernels  97.3 us (98%)
  local copies, waits for them, and re-layouts  1.67 us (2%)
    pallas_call x1, Pallas kernels, shards(): pl.pallas_call(functools.partial(layer_kernel, far, near, cores), out_sha...  97.3 us

profile of v2, /device:TPU:0, one launch (start us, length us, event | category | flops | bytes accessed | tf_op | source)
XLA Modules:
  0.0 99.0 jit_solution(16838546347438739416)
XLA Ops:
  0.0 97.3 %shard_map.172 = bf16[128,1024]{1,0:T(8,128)(2,1)} custom-call(bf16[128,512]{1,0:T(8,128)(2,1)} %q_in.1, bf16[128,512]{1,0:T(8,128)(2,1)} %v_in.1, bf16[128,512]{1,0:T(8,128)(2,1)} %f_in.1, bf16[128,512]{1,0:T(8,128)(2,1)} %r_in.1, bf16[128,512]{1,0:T(8,128)(2,1)} %og_in.1, f32[1,512]{1,0:T(1,128)} %bitcast.12, f32[1,512]{1,0:T(1,128)} %bitcast.13, ...), custom_call_target="tpu_custom_call" | custom-call | tf_op jit(solution)/shard_map/pallas_call | solution.py:569
  97.4 1.7 %copy.20 = bf16[128,1024]{1,0:T(8,128)(2,1)} copy(bf16[128,1024]{1,0:T(8,128)(2,1)} %shard_map.172) | data formatting | bytes 524288

commit v3 on v2

--- a/solution.py
+++ b/solution.py
@@ -126,13 +126,14 @@
 
     for load in loads.values():
         load.start()
-    loaded("gate", "up")
-    for i, ref in enumerate((gate_ref, up_ref)):
+    def turn(i, ref):
         whole = ref[...].astype(f32).T
         for j in range(far):
             wsend[j, i] = whole[j * units : (j + 1) * units].astype(bf16)
-    wbuf[p, z, 0] = wsend[z, 0]
-    wbuf[p, z, 1] = wsend[z, 1]
+        wbuf[p, z, i] = wsend[z, i]
+
+    loaded("gate")
+    turn(0, gate_ref)
     pl.semaphore_wait(barrier, len(peers))
 
     def deal_copy(g, peer, slot, e):
@@ -175,9 +176,11 @@
         came(half_r.at[k - 2 * far + 1], wbuf.at[0, 0, 2])
 
     g0, u0, d0 = 0, far, 2 * far
-    for g in range(2):
-        deal(g, 1)
+    deal(0, 1)
     ring_start(g0)
+    loaded("up")
+    turn(1, up_ref)
+    deal(1, 1)
 
     pairs = ((om_ref, om_all), (res_ref, res_all), (ig_ref, ig_all), (ib_ref, ib_all))
 
@@ -230,6 +233,7 @@
     st_recv[p] = st_send[p]
     tot_recv[p] = tot_send[p]
 
+    ring_start(u0)
     came(s1_r.at[0], st_recv.at[pl.ds(0, near - 1)])
     came(s1_r.at[1], tot_recv.at[pl.ds(0, near - 1)])
 
@@ -259,7 +263,7 @@
             for i in range(2):
                 start(far_copy(i, d, e), far_valid(d, e))
 
-    ring_start(u0)
+    ring_forward(g0)
 
     came(s2_r.at[0], f_recv.at[0, pl.ds(1, far - 1)])
     came(s2_r.at[1], ft_recv.at[0, pl.ds(1, far - 1)])
@@ -281,7 +285,6 @@
 
     deal(0, 2)
     deal(1, 2)
-    ring_forward(g0)
     ring_start(g0 + 1)
 
     came(s3_r.at[0], b_recv.at[pl.ds(0, near - 1)])
@@ -371,13 +374,13 @@
         line_step(1, i)
     deal(1, 3)
     ring_start(g0 + 3)
+    ring_forward(u0 + 2)
     line_step(2, 0)
-    ring_forward(u0 + 2)
+    ring_forward(g0 + 3)
     for i in range(1, pieces):
         line_step(2, i)
     deal(2, 1)
     ring_start(u0 + 3)
-    ring_forward(g0 + 3)
     ring_forward(u0 + 3)
     loaded("down")
     ring_start(d0)

time: 99.2 us -> 98.7 us (level)
  no operation moved by 1% of the time
where the time goes in v3:
time: 98.7 us; the launch traced here: 98.6 us
  Pallas kernels  96.9 us (98%)
  local copies, waits for them, and re-layouts  1.67 us (2%)
    pallas_call x1, Pallas kernels, shards(): pl.pallas_call(functools.partial(layer_kernel, far, near, cores), out_sha...  96.9 us

profile of v3, /device:TPU:0, one launch (start us, length us, event | category | flops | bytes accessed | tf_op | source)
XLA Modules:
  0.0 98.6 jit_solution(6689038984877032240)
XLA Ops:
  0.0 96.9 %shard_map.172 = bf16[128,1024]{1,0:T(8,128)(2,1)} custom-call(bf16[128,512]{1,0:T(8,128)(2,1)} %q_in.1, bf16[128,512]{1,0:T(8,128)(2,1)} %v_in.1, bf16[128,512]{1,0:T(8,128)(2,1)} %f_in.1, bf16[128,512]{1,0:T(8,128)(2,1)} %r_in.1, bf16[128,512]{1,0:T(8,128)(2,1)} %og_in.1, f32[1,512]{1,0:T(1,128)} %bitcast.12, f32[1,512]{1,0:T(1,128)} %bitcast.13, ...), custom_call_target="tpu_custom_call" | custom-call | tf_op jit(solution)/shard_map/pallas_call | solution.py:572
  96.9 1.7 %copy.20 = bf16[128,1024]{1,0:T(8,128)(2,1)} copy(bf16[128,1024]{1,0:T(8,128)(2,1)} %shard_map.172) | data formatting | bytes 524288

commit v4 on v3

--- a/solution.py
+++ b/solution.py
@@ -127,9 +127,9 @@
     for load in loads.values():
         load.start()
     def turn(i, ref):
-        whole = ref[...].astype(f32).T
+        whole = ref[...].T
         for j in range(far):
-            wsend[j, i] = whole[j * units : (j + 1) * units].astype(bf16)
+            wsend[j, i] = whole[j * units : (j + 1) * units]
         wbuf[p, z, i] = wsend[z, i]
 
     loaded("gate")
@@ -457,14 +457,13 @@
     for k in range(far):
         ring_forward(d0 + k)
         down(k, close)
+        if k + 2 < far:
+            ring_start(d0 + k + 2)
+        reduce(k, False)
         if k:
             ring_done(d0 + k - 1)
             down(k - 1, [opposite])
-        reduce(k, False)
-        if k:
             reduce(k - 1, True)
-        if k + 2 < far:
-            ring_start(d0 + k + 2)
     ring_done(d0 + far - 1)
     down(far - 1, [opposite])
     reduce(far - 1, True)

time: 98.7 us -> 99 us (level)
  no operation moved by 1% of the time
where the time goes in v4:
time: 99 us; the launch traced here: 98.9 us
  Pallas kernels  97.2 us (98%)
  local copies, waits for them, and re-layouts  1.67 us (2%)
    pallas_call x1, Pallas kernels, shards(): pl.pallas_call(functools.partial(layer_kernel, far, near, cores), out_sha...  97.2 us

profile of v4, /device:TPU:0, one launch (start us, length us, event | category | flops | bytes accessed | tf_op | source)
XLA Modules:
  0.0 98.9 jit_solution(2171242424519444244)
XLA Ops:
  0.0 97.2 %shard_map.172 = bf16[128,1024]{1,0:T(8,128)(2,1)} custom-call(bf16[128,512]{1,0:T(8,128)(2,1)} %q_in.1, bf16[128,512]{1,0:T(8,128)(2,1)} %v_in.1, bf16[128,512]{1,0:T(8,128)(2,1)} %f_in.1, bf16[128,512]{1,0:T(8,128)(2,1)} %r_in.1, bf16[128,512]{1,0:T(8,128)(2,1)} %og_in.1, f32[1,512]{1,0:T(1,128)} %bitcast.12, f32[1,512]{1,0:T(1,128)} %bitcast.13, ...), custom_call_target="tpu_custom_call" | custom-call | tf_op jit(solution)/shard_map/pallas_call | solution.py:571
  97.2 1.7 %copy.20 = bf16[128,1024]{1,0:T(8,128)(2,1)} copy(bf16[128,1024]{1,0:T(8,128)(2,1)} %shard_map.172) | data formatting | bytes 524288
